TPU v7x, 32 devices: a whole 2x2x4 slice. The times are simulated.
32 devices in a mesh: rep: 2 (over x), fs: 4 (over z), tp: 4 (over y, core).
Axes of the slice: x: 2, y: 2, z: 4, core: 2. Of those that a mesh axis runs over, the one named last changes fastest.
Arguments:
- tokens: bfloat16 [4096, 2048], P(('rep', 'fs', 'tp')), may hold values from -6 to 6
- mixer_gain: float32 [2048], replicated, may hold values from 0.1 to 1.9
- direct_weight: float32 [2048, 1024], P('fs', 'tp'), may hold values from -0.125 to 0.125
- direct_scale: float32 [1024], P('tp'), may hold values from 0.5 to 2
- value_weight: float32 [2048, 1024], P('fs', 'tp'), may hold values from -0.125 to 0.125
- value_scale: float32 [1024], P('tp'), may hold values from 0.5 to 8, as said below
- value_gain: float32 [1024], P('tp'), may hold values from 0.1 to 1.9
- value_shift: float32 [1024], P('tp'), may hold values from -3 to 3
- spatial_weight: bfloat16 [16, 128, 128], P('tp'), may hold values from -0.25 to 0.25
- spatial_bias: float32 [16, 128], P('tp'), may hold values from 0.1 to 1.9
- merge_weight: float32 [1024, 2048], P('tp', 'fs'), may hold values from -0.1875 to 0.1875
- merge_scale: float32 [2048], P('fs'), may hold values from 0.5 to 2
- channel_gain: float32 [2048], replicated, may hold values from 0.1 to 1.9
- expand_weight: float32 [2048, 8192], P('fs', 'tp'), may hold values from -0.125 to 0.125
- expand_scale: float32 [8192], P('tp'), may hold values from 0.5 to 2
- reduce_weight: float32 [8192, 2048], P('tp', 'fs'), may hold values from -0.0625 to 0.0625
- reduce_scale: float32 [2048], P('fs'), may hold values from 0.5 to 2
Outputs:
- result: bfloat16 [4096, 2048], P(('rep', 'fs', 'tp'))
Inputs may be any that keep to these rules, and one draw needn't show every extreme that they name: `value_scale`: positive column scales.
All inputs are finite; a program needn't handle non-finite values.
Results may differ from a plain program's by a relative error of at most 0.024.
Values may be sent and summed in bfloat16 or wider, within the bound.
A program may use at most 64 MiB of HBM per device.

v0:
```python
import jax
import jax.numpy as jnp
from jax import lax
from jax.sharding import PartitionSpec as P

GDIM = 64
BLOCK = 128
epsilon = 1e-06


def rms_rows(rows, gain):
    floats = rows.astype(jnp.float32)
    scaled = floats * lax.rsqrt(jnp.mean(floats * floats, axis=-1, keepdims=True) + epsilon)
    return (scaled * gain).astype(jnp.bfloat16)


def body(
    tokens,
    mixer_gain,
    direct_weight,
    direct_scale,
    value_weight,
    value_scale,
    value_gain,
    value_shift,
    spatial_weight,
    spatial_bias,
    merge_weight,
    merge_scale,
    channel_gain,
    expand_weight,
    expand_scale,
    reduce_weight,
    reduce_scale,
):
    direct_half = direct_weight.astype(jnp.bfloat16)
    value_half = value_weight.astype(jnp.bfloat16)
    merge_half = merge_weight.astype(jnp.bfloat16)
    expand_half = expand_weight.astype(jnp.bfloat16)
    reduce_half = reduce_weight.astype(jnp.bfloat16)
    full_expand, full_reduce, reduce_full_scale = (
        lax.all_gather(expand_half, "fs", axis=0, tiled=True),
        lax.all_gather(reduce_half, "fs", axis=1, tiled=True),
        lax.all_gather(reduce_scale.astype(jnp.bfloat16), "fs", axis=0, tiled=True).astype(
            reduce_scale.dtype
        ),
    )
    normed = rms_rows(tokens, mixer_gain)
    whole = lax.all_gather(normed, "tp", axis=0, tiled=True)
    seq_rows = whole.shape[0]
    local_width = direct_weight.shape[1]
    direct_pre = jnp.dot(
        whole,
        lax.all_gather(direct_half, "fs", axis=0, tiled=True),
        preferred_element_type=jnp.float32,
    )
    value_pre = jnp.dot(
        whole,
        lax.all_gather(value_half, "fs", axis=0, tiled=True),
        preferred_element_type=jnp.float32,
    )
    full_merge, merge_full_scale = (
        lax.all_gather(merge_half, "fs", axis=1, tiled=True),
        lax.all_gather(merge_scale.astype(jnp.bfloat16), "fs", axis=0, tiled=True).astype(
            merge_scale.dtype
        ),
    )
    direct = jax.nn.gelu(direct_pre * direct_scale)
    value = jax.nn.gelu(value_pre * value_scale)
    total, squares = lax.psum((jnp.sum(value, axis=1), jnp.sum(value * value, axis=1)), "tp")
    branch_width = local_width * lax.axis_size("tp")
    mean = (total / branch_width)[:, None]
    var = (squares / branch_width)[:, None] - mean * mean
    gated_value = ((value - mean) * lax.rsqrt(var + epsilon) * value_gain + value_shift).astype(
        jnp.bfloat16
    )
    local_groups = spatial_weight.shape[0]
    blocks = gated_value.reshape(seq_rows // BLOCK, BLOCK, local_groups, GDIM)
    mixed = jnp.einsum("gpq,nqgc->npgc", spatial_weight, blocks, preferred_element_type=jnp.float32)
    mixed = mixed + jnp.transpose(spatial_bias)[None, :, :, None]
    gated = (direct * mixed.reshape(seq_rows, local_width)).astype(jnp.bfloat16)
    rows = gated
    mix = lax.psum_scatter(
        (jnp.dot(rows, full_merge, preferred_element_type=jnp.float32) * merge_full_scale).astype(
            jnp.bfloat16
        ),
        "tp",
        scatter_dimension=0,
        tiled=True,
    ).astype(jnp.float32)
    middle = (tokens.astype(jnp.float32) + mix).astype(jnp.bfloat16)
    normed_mid = rms_rows(middle, channel_gain)
    whole_mid = lax.all_gather(normed_mid, "tp", axis=0, tiled=True)
    upper = jnp.dot(whole_mid, full_expand, preferred_element_type=jnp.float32)
    hidden = jnp.square(jax.nn.relu(upper * expand_scale)).astype(jnp.bfloat16)
    rows = hidden
    lower = lax.psum_scatter(
        (jnp.dot(rows, full_reduce, preferred_element_type=jnp.float32) * reduce_full_scale).astype(
            jnp.bfloat16
        ),
        "tp",
        scatter_dimension=0,
        tiled=True,
    ).astype(jnp.float32)
    return (middle.astype(jnp.float32) + lower).astype(jnp.bfloat16)


def solution(mesh):
    return jax.shard_map(
        body,
        mesh=mesh,
        in_specs=(
            P(("rep", "fs", "tp"), None),
            P(),
            P("fs", "tp"),
            P("tp"),
            P("fs", "tp"),
            P("tp"),
            P("tp"),
            P("tp"),
            P("tp", None, None),
            P("tp", None),
            P("tp", "fs"),
            P("fs"),
            P(),
            P("fs", "tp"),
            P("tp"),
            P("tp", "fs"),
            P("fs"),
        ),
        out_specs=P(("rep", "fs", "tp"), None),
        check_vma=False,
    )
```

profile of v0, /device:TPU:0, one launch (start us, length us, event | category | flops | bytes accessed | tf_op | source)
XLA Modules:
  0.0 539.8 jit_solution(16502499518747901413)
XLA Ops:
  6.6 1.8 convert_element_type.71
  8.5 1.2 fusion.1
  9.7 2.0 fusion.3
  11.8 1.8 convert_element_type.70
  14.5 13.9 %all-gather = bf16[4,1,512]{2,1,0:T(2,128)(2,1)S(1)} all-gather(bf16[1,1,512]{2,1,0:T(2,128)(2,1)S(1)} %reshape.40), channel_id=1, replica_groups=mesh['rep'=2,'fs'=4,'tp'=4] {'fs'}, dimensions={0}, use_global_device_ids=true | all-gather | bytes 5120 | tf_op jit(solution)/shard_map/all_gather | solution.py:64
  28.4 11.3 %all-gather.14.cloned.1.call-done = bf16[2048,256]{1,0:T(8,128)(2,1)} async-done(((bf16[512,256]{1,0:T(8,128)(2,1)}), bf16[2048,256]{1,0:T(8,128)(2,1)}) %all-gather.14.cloned.1.call-update) | async-done | bytes 1048592 | tf_op jit(solution)/shard_map/all_gather | solution.py:59
  39.7 23.5 %all-gather.10.cloned.1.call-done = bf16[512,2048]{1,0:T(8,128)(2,1)} async-done(((bf16[128,2048]{1,0:T(8,128)(2,1)}), bf16[512,2048]{1,0:T(8,128)(2,1)}) %all-gather.10.cloned.1.call-update) | async-done | bytes 2097168 | tf_op jit(solution)/shard_map/all_gather | solution.py:49
  63.3 2.8 fusion.37
  66.1 5.9 %all-reduce = (f32[512]{0:T(512)S(1)}, f32[512]{0:T(512)S(1)}) all-reduce(f32[512]{0:T(512)S(1)} %get-tuple-element.6, f32[512]{0:T(512)S(1)} %get-tuple-element.5), channel_id=1, replica_groups=mesh['rep'=2,'fs'=4,'tp'=4] {'tp'}, use_global_device_ids=true, to_apply=%region_4.0 | all-reduce | flops 1024 | bytes 8192 | tf_op jit(solution)/shard_map/psum | solution.py:70
  73.8 19.1 %all-gather.12.cloned.1.call-done = bf16[2048,256]{1,0:T(8,128)(2,1)} async-done(((bf16[512,256]{1,0:T(8,128)(2,1)}), bf16[2048,256]{1,0:T(8,128)(2,1)}) %all-gather.12.cloned.1.call-update) | async-done | bytes 1048592 | tf_op jit(solution)/shard_map/all_gather | solution.py:54
  92.9 28.8 %all-gather.16.cloned.1.call-done = bf16[256,2048]{1,0:T(8,128)(2,1)} async-done(((bf16[256,512]{1,0:T(8,128)(2,1)}), bf16[256,2048]{1,0:T(8,128)(2,1)}) %all-gather.16.cloned.1.call-update) | async-done | bytes 1048592 | tf_op jit(solution)/shard_map/all_gather | solution.py:63
  121.7 5.9 %multiply_convert_fusion.2 = bf16[512,2048]{1,0:T(8,128)(2,1)} fusion(bf16[256,2048]{1,0:T(8,128)(2,1)} %all-gather.16.cloned.1.call-done, f32[2048]{0:T(1024)S(1)} %bitcast.20, f32[512,256]{1,0:T(8,128)S(1)} %reshape.48, bf16[512,2048]{1,0:T(8,128)(2,1)} %all-gather.10.cloned.1.call-done, bf16[2048,256]{1,0:T(8,128)(2,1)} %all-gather.12.cloned.1.call-done, ...), kind=kOutput, calls=%fused_computation.2 | convolution fusion | flops 1077280768 | bytes 6824960 | tf_op jit(solution)/shard_map/dot_general | solution.py:84
  127.7 30.7 %reduce-scatter.3.cloned.1.call-done = bf16[128,2048]{1,0:T(8,128)(2,1)} async-done(((bf16[512,2048]{1,0:T(8,128)(2,1)}), bf16[128,2048]{1,0:T(8,128)(2,1)}) %reduce-scatter.3.cloned.1.call-update) | async-done | bytes 524304 | tf_op jit(solution)/shard_map/reduce_scatter | solution.py:83
  158.3 1.3 fusion.5
  159.7 2.0 fusion.7
  161.8 3.8 convert_element_type.82
  165.7 3.9 convert_element_type.84
  169.6 12.1 %all-gather.1 = bf16[4,1,512]{2,1,0:T(2,128)(2,1)S(1)} all-gather(bf16[1,1,512]{2,1,0:T(2,128)(2,1)S(1)} %reshape.42), channel_id=1, replica_groups=mesh['rep'=2,'fs'=4,'tp'=4] {'fs'}, dimensions={0}, use_global_device_ids=true | all-gather | bytes 5120 | tf_op jit(solution)/shard_map/all_gather | solution.py:44
  181.8 2.7 all-gather.18.cloned.1.call-done
  184.4 151.2 %all-gather.20.cloned.1.call-done = bf16[2048,2048]{1,0:T(8,128)(2,1)} async-done(((bf16[512,2048]{1,0:T(8,128)(2,1)}), bf16[2048,2048]{1,0:T(8,128)(2,1)}) %all-gather.20.cloned.1.call-update) | async-done | bytes 8388624 | tf_op jit(solution)/shard_map/all_gather | solution.py:42
  335.7 149.4 %all-gather.22.cloned.1.call-done = bf16[2048,2048]{1,0:T(8,128)(2,1)} async-done(((bf16[2048,512]{1,0:T(8,128)(2,1)}), bf16[2048,2048]{1,0:T(8,128)(2,1)}) %all-gather.22.cloned.1.call-update) | async-done | bytes 8388624 | tf_op jit(solution)/shard_map/all_gather | solution.py:43
  485.1 16.6 %multiply_convert_fusion = bf16[512,2048]{1,0:T(8,128)(2,1)} fusion(bf16[2048,2048]{1,0:T(8,128)(2,1)} %all-gather.22.cloned.1.call-done, f32[2048]{0:T(1024)S(1)} %bitcast.21, bf16[512,2048]{1,0:T(8,128)(2,1)} %all-gather.18.cloned.1.call-done, bf16[2048,2048]{1,0:T(8,128)(2,1)} %all-gather.20.cloned.1.call-done, f32[2048]{0:T(1024)S(1)} %copy-done.10), kind=kOutput, calls=%fused_computation | convolution fusion | flops 8596226048 | bytes 20987904 | tf_op jit(solution)/shard_map/dot_general | solution.py:98
  501.6 29.5 %reduce-scatter.5.cloned.1.call-done = bf16[128,2048]{1,0:T(8,128)(2,1)} async-done(((bf16[512,2048]{1,0:T(8,128)(2,1)}), bf16[128,2048]{1,0:T(8,128)(2,1)}) %reduce-scatter.5.cloned.1.call-update) | async-done | bytes 524304 | tf_op jit(solution)/shard_map/reduce_scatter | solution.py:97
  531.2 2.1 fusion.8
  (59 shorter events, 3.1 us)
Async XLA Ops:
  6.5 65.9 %copy-start = (bf16[4,128,128]{2,1,0:T(8,128)(2,1)S(1)}, bf16[4,128,128]{2,1,0:T(8,128)(2,1)}, u32[]{:S(2)}) copy-start(bf16[4,128,128]{2,1,0:T(8,128)(2,1)} %param.25) | copy-start | bytes 393220
  6.5 7.1 %copy-start.3 = (f32[256,512]{1,0:T(8,128)S(1)}, f32[256,512]{1,0:T(8,128)}, u32[]{:S(2)}) copy-start(f32[256,512]{1,0:T(8,128)} %param.27) | copy-start | bytes 1572868
  6.5 7.9 %copy-start.6 = (f32[512]{0:T(512)S(1)}, f32[512]{0:T(512)}, u32[]{:S(2)}) copy-start(f32[512]{0:T(512)} %param.28) | copy-start | bytes 6148
  6.5 56.7 %copy-start.11 = (f32[256]{0:T(256)S(1)}, f32[256]{0:T(256)}, u32[]{:S(2)}) copy-start(f32[256]{0:T(256)} %param.22) | copy-start | bytes 3076
  6.5 33.2 %all-gather.14.cloned.1.call-start = ((), (), s32[]{:S(2)}) async-start(), calls=%async_computation.4 | async-start | bytes 1310720 | tf_op jit(solution)/shard_map/all_gather | solution.py:59
  8.4 54.8 %all-gather.10.cloned.1.call-start = ((), (), s32[]{:S(2)}) async-start(), calls=%async_computation.2 | async-start | bytes 2621440 | tf_op jit(solution)/shard_map/all_gather | solution.py:49
  11.8 81.1 %all-gather.12.cloned.1.call-start = ((), (), s32[]{:S(2)}) async-start(), calls=%async_computation.3 | async-start | bytes 1310720 | tf_op jit(solution)/shard_map/all_gather | solution.py:54
  13.6 108.1 %all-gather.16.cloned.1.call-start = ((), (), s32[]{:S(2)}) async-start(), calls=%async_computation.5 | async-start | bytes 1310720 | tf_op jit(solution)/shard_map/all_gather | solution.py:63
  14.4 57.6 %copy-start.8 = (f32[256]{0:T(256)S(1)}, f32[256]{0:T(256)}, u32[]{:S(2)}) copy-start(f32[256]{0:T(256)} %param.24) | copy-start | bytes 3076
  14.4 57.6 %copy-start.9 = (f32[256]{0:T(256)S(1)}, f32[256]{0:T(256)}, u32[]{:S(2)}) copy-start(f32[256]{0:T(256)} %param.23) | copy-start | bytes 3076
  14.4 143.9 %reduce-scatter.3.cloned.1.call-start = ((), (), s32[]{:S(2)}) async-start(), calls=%async_computation.6 | async-start | bytes 2621440 | tf_op jit(solution)/shard_map/reduce_scatter | solution.py:83
  28.4 44.0 %copy-start.5 = (f32[4,128]{1,0:T(4,128)S(1)}, f32[4,128]{1,0:T(4,128)}, u32[]{:S(2)}) copy-start(f32[4,128]{1,0:T(4,128)} %param.26) | copy-start | bytes 6148
  66.1 55.6 %copy-start.12 = (f32[256]{0:T(256)S(1)}, f32[256]{0:T(256)}, u32[]{:S(2)}) copy-start(f32[256]{0:T(256)} %param.20) | copy-start | bytes 3076
  121.7 36.7 %copy-start.1 = (bf16[128,2048]{1,0:T(8,128)(2,1)S(1)}, bf16[128,2048]{1,0:T(8,128)(2,1)}, u32[]{:S(2)}) copy-start(bf16[128,2048]{1,0:T(8,128)(2,1)} %param.17) | copy-start | bytes 1572868
  121.7 38.0 %copy-start.4 = (f32[2048]{0:T(1024)S(1)}, f32[2048]{0:T(1024)}, u32[]{:S(2)}) copy-start(f32[2048]{0:T(1024)} %param.29) | copy-start | bytes 24580
  127.6 56.8 %all-gather.18.cloned.1.call-start = ((), (), s32[]{:S(2)}) async-start(), calls=%async_computation.7 | async-start | bytes 2621440 | tf_op jit(solution)/shard_map/all_gather | solution.py:93
  161.7 173.9 %all-gather.20.cloned.1.call-start = ((), (), s32[]{:S(2)}) async-start(), calls=%async_computation.8 | async-start | bytes 10485760 | tf_op jit(solution)/shard_map/all_gather | solution.py:42
  165.6 4.0 copy-start.7
  165.6 319.4 %copy-start.10 = (f32[2048]{0:T(1024)S(1)}, f32[2048]{0:T(1024)}, u32[]{:S(2)}) copy-start(f32[2048]{0:T(1024)} %param.31) | copy-start | bytes 24580
  165.6 319.4 %all-gather.22.cloned.1.call-start = ((), (), s32[]{:S(2)}) async-start(), calls=%async_computation.9 | async-start | bytes 10485760 | tf_op jit(solution)/shard_map/all_gather | solution.py:43
  169.6 361.6 %reduce-scatter.5.cloned.1.call-start = ((), (), s32[]{:S(2)}) async-start(), calls=%async_computation.10 | async-start | bytes 2621440 | tf_op jit(solution)/shard_map/reduce_scatter | solution.py:97
  485.0 46.1 %copy-start.2 = (bf16[128,2048]{1,0:T(8,128)(2,1)S(1)}, bf16[128,2048]{1,0:T(8,128)(2,1)}, u32[]{:S(2)}) copy-start(bf16[128,2048]{1,0:T(8,128)(2,1)} %reduce-scatter.3.cloned.1.call-done) | copy-start | bytes 1572868
Sparse Core Ops, SparseCore 0:
  8.9 30.7 all-gather.13
  41.3 21.9 all-gather.9
  64.9 27.9 all-gather.11
  94.3 27.3 all-gather.15
  127.7 30.5 reduce-scatter.2
  161.8 22.5 all-gather.17
  186.0 149.5 all-gather.19
  337.2 147.7 all-gather.21
  501.8 29.3 reduce-scatter.4
where the time goes:
time: 540 us
  waiting for transfers between devices  446 us (83%)
  blocking collectives  31.9 us (6%)
  matrix products  25.6 us (5%)
  other arithmetic  20.9 us (4%)
  between operations  13.4 us (2%)
    all_gather x1, waiting for transfers between devices, body(): lax.all_gather(expand_half, 'fs', axis=0, tiled=True)  151 us
    all_gather x1, waiting for transfers between devices, body(): lax.all_gather(reduce_half, 'fs', axis=1, tiled=True)  149 us
    reduce_scatter x1, waiting for transfers between devices, body(): lax.psum_scatter((jnp.dot(rows, full_merge, preferred_element_type=jnp.fl...  30.7 us
    reduce_scatter x1, waiting for transfers between devices, body(): lax.psum_scatter((jnp.dot(rows, full_reduce, preferred_element_type=jnp.f...  29.5 us
    all_gather x1, waiting for transfers between devices, body(): lax.all_gather(merge_half, 'fs', axis=1, tiled=True)  28.8 us
    all_gather x1, waiting for transfers between devices, body(): whole = lax.all_gather(normed, 'tp', axis=0, tiled=True)  23.5 us
    all_gather x1, waiting for transfers between devices, body(): lax.all_gather(direct_half, 'fs', axis=0, tiled=True)  19.1 us
    dot_general x1, matrix products, body(): jnp.dot(rows, full_reduce, preferred_element_type=jnp.float32)  16.6 us
  transfers between devices with their start and end apart: 9, of which 9 were waited for; matrix products, arithmetic and copies ran while one was open for 3% of the time, Pallas kernels for 0%

commit v1 on v0

--- a/solution.py
+++ b/solution.py
@@ -1,3 +1,4 @@
+import functools
 import jax
 import jax.numpy as jnp
 from jax import lax
@@ -6,6 +7,14 @@
 GDIM = 64
 BLOCK = 128
 epsilon = 1e-06
+
+
+def _draw_cycles(buf, mesh_dim):
+    left_arr = jnp.concatenate(lax.all_gather(buf, mesh_dim), 1)
+    return left_arr
+
+
+racks_detail = functools.partial(_draw_cycles, mesh_dim="fs")
 
 
 def rms_rows(rows, gain):
@@ -60,7 +69,7 @@
         preferred_element_type=jnp.float32,
     )
     full_merge, merge_full_scale = (
-        lax.all_gather(merge_half, "fs", axis=1, tiled=True),
+        racks_detail(merge_half),
         lax.all_gather(merge_scale.astype(jnp.bfloat16), "fs", axis=0, tiled=True).astype(
             merge_scale.dtype
         ),

time: 540 us -> 540 us (level)
    all_gather x1, waiting for transfers between devices: 28.8 us -> 11.3 us  [_draw_cycles(): left_arr = jnp.concatenate(lax.all_gather(buf, mesh_dim), 1)]
    all_gather x1, waiting for transfers between devices: 11.3 us -> 27.4 us  [body(): lax.all_gather(value_half, 'fs', axis=0, tiled=True)]
  transfers between devices with their start and end apart: 9 -> 9, of which waited for: 9 -> 9; matrix products, arithmetic and copies ran while one was open for 3% -> 4% of each run, Pallas kernels for 0% -> 0%
where the time goes in v1:
time: 540 us; the launch traced here: 539 us
  waiting for transfers between devices  445 us (82%)
  blocking collectives  31.9 us (6%)
  matrix products  25.2 us (5%)
  other arithmetic  20.9 us (4%)
  between operations  13.4 us (2%)
    all_gather x1, waiting for transfers between devices, body(): lax.all_gather(expand_half, 'fs', axis=0, tiled=True)  151 us
    all_gather x1, waiting for transfers between devices, body(): lax.all_gather(reduce_half, 'fs', axis=1, tiled=True)  149 us
    reduce_scatter x1, waiting for transfers between devices, body(): lax.psum_scatter((jnp.dot(rows, full_merge, preferred_element_type=jnp.fl...  30.7 us
    reduce_scatter x1, waiting for transfers between devices, body(): lax.psum_scatter((jnp.dot(rows, full_reduce, preferred_element_type=jnp.f...  29.5 us
    all_gather x1, waiting for transfers between devices, body(): lax.all_gather(value_half, 'fs', axis=0, tiled=True)  27.4 us
    all_gather x1, waiting for transfers between devices, body(): whole = lax.all_gather(normed, 'tp', axis=0, tiled=True)  23.5 us
    all_gather x1, waiting for transfers between devices, body(): lax.all_gather(direct_half, 'fs', axis=0, tiled=True)  18.9 us
    dot_general x1, matrix products, body(): jnp.dot(rows, full_reduce, preferred_element_type=jnp.float32)  16.6 us
  transfers between devices with their start and end apart: 9, of which 9 were waited for; matrix products, arithmetic and copies ran while one was open for 4% of the time, Pallas kernels for 0%

profile of v1, /device:TPU:0, one launch (start us, length us, event | category | flops | bytes accessed | tf_op | source)
XLA Modules:
  0.0 539.4 jit_solution(17999194710954520992)
XLA Ops:
  6.6 1.8 convert_element_type.74
  8.5 1.8 convert_element_type.71
  11.6 2.0 fusion.3
  14.5 13.9 %all-gather.1 = bf16[4,1,512]{2,1,0:T(2,128)(2,1)S(1)} all-gather(bf16[1,1,512]{2,1,0:T(2,128)(2,1)S(1)} %reshape.49), channel_id=1, replica_groups=mesh['rep'=2,'fs'=4,'tp'=4] {'fs'}, dimensions={0}, use_global_device_ids=true | all-gather | bytes 5120 | tf_op jit(solution)/shard_map/all_gather | solution.py:73
  28.4 11.3 %all-gather.23.cloned.1.call-done = bf16[1024,512]{1,0:T(8,128)(2,1)} async-done(((bf16[256,512]{1,0:T(8,128)(2,1)}), bf16[1024,512]{1,0:T(8,128)(2,1)}) %all-gather.23.cloned.1.call-update) | async-done | bytes 1048592 | tf_op jit(solution)/shard_map/all_gather | solution.py:13
  39.7 1.5 copy.37
  41.3 27.4 %all-gather.15.cloned.1.call-done = bf16[2048,256]{1,0:T(8,128)(2,1)} async-done(((bf16[512,256]{1,0:T(8,128)(2,1)}), bf16[2048,256]{1,0:T(8,128)(2,1)}) %all-gather.15.cloned.1.call-update) | async-done | bytes 1048592 | tf_op jit(solution)/shard_map/all_gather | solution.py:68
  68.7 23.5 %all-gather.11.cloned.1.call-done = bf16[512,2048]{1,0:T(8,128)(2,1)} async-done(((bf16[128,2048]{1,0:T(8,128)(2,1)}), bf16[512,2048]{1,0:T(8,128)(2,1)}) %all-gather.11.cloned.1.call-update) | async-done | bytes 2097168 | tf_op jit(solution)/shard_map/all_gather | solution.py:58
  92.2 2.8 fusion.37
  95.0 5.9 %all-reduce = (f32[512]{0:T(512)S(1)}, f32[512]{0:T(512)S(1)}) all-reduce(f32[512]{0:T(512)S(1)} %get-tuple-element.6, f32[512]{0:T(512)S(1)} %get-tuple-element.5), channel_id=1, replica_groups=mesh['rep'=2,'fs'=4,'tp'=4] {'tp'}, use_global_device_ids=true, to_apply=%region_4.0 | all-reduce | flops 1024 | bytes 8192 | tf_op jit(solution)/shard_map/psum | solution.py:79
  102.8 18.9 %all-gather.13.cloned.1.call-done = bf16[2048,256]{1,0:T(8,128)(2,1)} async-done(((bf16[512,256]{1,0:T(8,128)(2,1)}), bf16[2048,256]{1,0:T(8,128)(2,1)}) %all-gather.13.cloned.1.call-update) | async-done | bytes 1048592 | tf_op jit(solution)/shard_map/all_gather | solution.py:63
  121.7 5.6 %multiply_convert_fusion.2 = bf16[512,2048]{1,0:T(8,128)(2,1)} fusion(bf16[256,2048]{0,1:T(8,128)(2,1)S(1)} %bitcast.25, f32[2048]{0:T(1024)S(1)} %bitcast.26, f32[512,256]{1,0:T(8,128)S(1)} %reshape.57, bf16[512,2048]{1,0:T(8,128)(2,1)} %all-gather.11.cloned.1.call-done, bf16[2048,256]{1,0:T(8,128)(2,1)} %all-gather.13.cloned.1.call-done, f32[256]{0:T(256)S(1)} %copy-done.12), kind=kOutput, calls=%fused_computation.2 | convolution fusion | flops 1077280768 | bytes 6824960 | tf_op jit(solution)/shard_map/dot_general | solution.py:93
  127.4 30.7 %reduce-scatter.3.cloned.1.call-done = bf16[128,2048]{1,0:T(8,128)(2,1)} async-done(((bf16[512,2048]{1,0:T(8,128)(2,1)}), bf16[128,2048]{1,0:T(8,128)(2,1)}) %reduce-scatter.3.cloned.1.call-update) | async-done | bytes 524304 | tf_op jit(solution)/shard_map/reduce_scatter | solution.py:92
  158.0 1.3 fusion.5
  159.3 2.0 fusion.7
  161.5 3.8 convert_element_type.82
  165.4 3.9 convert_element_type.84
  169.3 12.1 %all-gather.2 = bf16[4,1,512]{2,1,0:T(2,128)(2,1)S(1)} all-gather(bf16[1,1,512]{2,1,0:T(2,128)(2,1)S(1)} %reshape.51), channel_id=1, replica_groups=mesh['rep'=2,'fs'=4,'tp'=4] {'fs'}, dimensions={0}, use_global_device_ids=true | all-gather | bytes 5120 | tf_op jit(solution)/shard_map/all_gather | solution.py:53
  181.5 2.7 all-gather.17.cloned.1.call-done
  184.1 151.2 %all-gather.19.cloned.1.call-done = bf16[2048,2048]{1,0:T(8,128)(2,1)} async-done(((bf16[512,2048]{1,0:T(8,128)(2,1)}), bf16[2048,2048]{1,0:T(8,128)(2,1)}) %all-gather.19.cloned.1.call-update) | async-done | bytes 8388624 | tf_op jit(solution)/shard_map/all_gather | solution.py:51
  335.3 149.4 %all-gather.21.cloned.1.call-done = bf16[2048,2048]{1,0:T(8,128)(2,1)} async-done(((bf16[2048,512]{1,0:T(8,128)(2,1)}), bf16[2048,2048]{1,0:T(8,128)(2,1)}) %all-gather.21.cloned.1.call-update) | async-done | bytes 8388624 | tf_op jit(solution)/shard_map/all_gather | solution.py:52
  484.7 16.6 %multiply_convert_fusion = bf16[512,2048]{1,0:T(8,128)(2,1)} fusion(bf16[2048,2048]{1,0:T(8,128)(2,1)} %all-gather.21.cloned.1.call-done, f32[2048]{0:T(1024)S(1)} %bitcast.27, bf16[512,2048]{1,0:T(8,128)(2,1)} %all-gather.17.cloned.1.call-done, bf16[2048,2048]{1,0:T(8,128)(2,1)} %all-gather.19.cloned.1.call-done, f32[2048]{0:T(1024)S(1)} %copy-done.10), kind=kOutput, calls=%fused_computation | convolution fusion | flops 8596226048 | bytes 20987904 | tf_op jit(solution)/shard_map/dot_general | solution.py:107
  501.3 29.5 %reduce-scatter.5.cloned.1.call-done = bf16[128,2048]{1,0:T(8,128)(2,1)} async-done(((bf16[512,2048]{1,0:T(8,128)(2,1)}), bf16[128,2048]{1,0:T(8,128)(2,1)}) %reduce-scatter.5.cloned.1.call-update) | async-done | bytes 524304 | tf_op jit(solution)/shard_map/reduce_scatter | solution.py:106
  530.8 2.1 fusion.8
  (60 shorter events, 4.4 us)
Async XLA Ops:
  6.5 94.9 %copy-start = (bf16[4,128,128]{2,1,0:T(8,128)(2,1)S(1)}, bf16[4,128,128]{2,1,0:T(8,128)(2,1)}, u32[]{:S(2)}) copy-start(bf16[4,128,128]{2,1,0:T(8,128)(2,1)} %param.25) | copy-start | bytes 393220
  6.5 7.2 %copy-start.3 = (f32[512,256]{1,0:T(8,128)S(1)}, f32[512,256]{1,0:T(8,128)}, u32[]{:S(2)}) copy-start(f32[512,256]{1,0:T(8,128)} %param.19) | copy-start | bytes 1572868
  6.5 8.0 %copy-start.6 = (f32[512]{0:T(512)S(1)}, f32[512]{0:T(512)}, u32[]{:S(2)}) copy-start(f32[512]{0:T(512)} %param.28) | copy-start | bytes 6148
  6.5 85.7 %copy-start.11 = (f32[256]{0:T(256)S(1)}, f32[256]{0:T(256)}, u32[]{:S(2)}) copy-start(f32[256]{0:T(256)} %param.22) | copy-start | bytes 3076
  6.5 33.2 %all-gather.23.cloned.1.call-start = ((), (), s32[]{:S(2)}) async-start(), calls=%async_computation.10 | async-start | bytes 1310720 | tf_op jit(solution)/shard_map/all_gather | solution.py:13
  8.5 60.2 %all-gather.15.cloned.1.call-start = ((), (), s32[]{:S(2)}) async-start(), calls=%async_computation.4 | async-start | bytes 1310720 | tf_op jit(solution)/shard_map/all_gather | solution.py:68
  10.3 81.9 %all-gather.11.cloned.1.call-start = ((), (), s32[]{:S(2)}) async-start(), calls=%async_computation.2 | async-start | bytes 2621440 | tf_op jit(solution)/shard_map/all_gather | solution.py:58
  13.6 108.0 %all-gather.13.cloned.1.call-start = ((), (), s32[]{:S(2)}) async-start(), calls=%async_computation.3 | async-start | bytes 1310720 | tf_op jit(solution)/shard_map/all_gather | solution.py:63
  14.4 143.6 %reduce-scatter.3.cloned.1.call-start = ((), (), s32[]{:S(2)}) async-start(), calls=%async_computation.5 | async-start | bytes 2621440 | tf_op jit(solution)/shard_map/reduce_scatter | solution.py:92
  41.2 59.7 %copy-start.8 = (f32[256]{0:T(256)S(1)}, f32[256]{0:T(256)}, u32[]{:S(2)}) copy-start(f32[256]{0:T(256)} %param.24) | copy-start | bytes 3076
  41.2 59.7 %copy-start.9 = (f32[256]{0:T(256)S(1)}, f32[256]{0:T(256)}, u32[]{:S(2)}) copy-start(f32[256]{0:T(256)} %param.23) | copy-start | bytes 3076
  41.2 60.2 %copy-start.5 = (f32[4,128]{1,0:T(4,128)S(1)}, f32[4,128]{1,0:T(4,128)}, u32[]{:S(2)}) copy-start(f32[4,128]{1,0:T(4,128)} %param.26) | copy-start | bytes 6148
  95.0 26.7 %copy-start.12 = (f32[256]{0:T(256)S(1)}, f32[256]{0:T(256)}, u32[]{:S(2)}) copy-start(f32[256]{0:T(256)} %param.20) | copy-start | bytes 3076
  121.7 36.3 %copy-start.1 = (bf16[128,2048]{1,0:T(8,128)(2,1)S(1)}, bf16[128,2048]{1,0:T(8,128)(2,1)}, u32[]{:S(2)}) copy-start(bf16[128,2048]{1,0:T(8,128)(2,1)} %param.17) | copy-start | bytes 1572868
  121.7 37.6 %copy-start.4 = (f32[2048]{0:T(1024)S(1)}, f32[2048]{0:T(1024)}, u32[]{:S(2)}) copy-start(f32[2048]{0:T(1024)} %param.29) | copy-start | bytes 24580
  127.3 56.8 %all-gather.17.cloned.1.call-start = ((), (), s32[]{:S(2)}) async-start(), calls=%async_computation.6 | async-start | bytes 2621440 | tf_op jit(solution)/shard_map/all_gather | solution.py:102
  161.4 173.9 %all-gather.19.cloned.1.call-start = ((), (), s32[]{:S(2)}) async-start(), calls=%async_computation.7 | async-start | bytes 10485760 | tf_op jit(solution)/shard_map/all_gather | solution.py:51
  165.3 4.0 copy-start.7
  165.3 319.4 %copy-start.10 = (f32[2048]{0:T(1024)S(1)}, f32[2048]{0:T(1024)}, u32[]{:S(2)}) copy-start(f32[2048]{0:T(1024)} %param.31) | copy-start | bytes 24580
  165.3 319.4 %all-gather.21.cloned.1.call-start = ((), (), s32[]{:S(2)}) async-start(), calls=%async_computation.8 | async-start | bytes 10485760 | tf_op jit(solution)/shard_map/all_gather | solution.py:52
  169.2 361.6 %reduce-scatter.5.cloned.1.call-start = ((), (), s32[]{:S(2)}) async-start(), calls=%async_computation.9 | async-start | bytes 2621440 | tf_op jit(solution)/shard_map/reduce_scatter | solution.py:106
  484.7 46.1 %copy-start.2 = (bf16[128,2048]{1,0:T(8,128)(2,1)S(1)}, bf16[128,2048]{1,0:T(8,128)(2,1)}, u32[]{:S(2)}) copy-start(bf16[128,2048]{1,0:T(8,128)(2,1)} %reduce-scatter.3.cloned.1.call-done) | copy-start | bytes 1572868
Sparse Core Ops, SparseCore 0:
  8.9 30.7 all-gather.22
  41.3 27.3 all-gather.14
  70.3 21.9 all-gather.10
  93.7 27.9 all-gather.12
  127.4 30.5 reduce-scatter.2
  161.5 22.5 all-gather.16
  185.7 149.5 all-gather.18
  336.9 147.7 all-gather.20
  501.4 29.3 reduce-scatter.4
